TPU v7x, 32 devices: a whole 2x2x4 slice. The times are simulated.
32 devices in a mesh: ep: 8 (over z, x), tp: 4 (over y, core).
Axes of the slice: x: 2, y: 2, z: 4, core: 2. Of those that a mesh axis runs over, the one named last changes fastest.
Arguments:
- tokens: bfloat16 [256, 4096], P('ep'), may hold values from -6 to 6
- mix_gain: bfloat16 [4096], replicated, may hold values from 0.099609375 to 1.8984375
- query_weight: bfloat16 [4096, 1024], P(None, 'tp'), may hold values from -0.09375 to 0.09375
- key_weight: bfloat16 [4096, 1024], P(None, 'tp'), may hold values from -0.09375 to 0.09375
- value_weight: bfloat16 [4096, 1024], P(None, 'tp'), may hold values from -0.09375 to 0.09375
- decay_weight: bfloat16 [4096, 8], replicated, may hold values from -0.09375 to 0.09375
- strength_weight: bfloat16 [4096, 8], replicated, may hold values from -0.09375 to 0.09375
- decay_rate: float32 [8], P('tp'), may hold values from 0.03 to 3
- head_gain: bfloat16 [128], replicated, may hold values from 0.099609375 to 1.8984375
- memory_state: float32 [256, 8, 128, 128], P('ep', 'tp'), may hold values from -0.6 to 0.6
- output_weight: bfloat16 [1024, 4096], P('tp'), may hold values from -0.1875 to 0.1875
- ffn_gain: bfloat16 [4096], replicated, may hold values from 0.099609375 to 1.8984375
- routing: int32 [256, 2], P('ep'), may hold values from 0 to 7, all different within a row; in each aligned block of 32 rows (0 to 31, 32 to 63, ...) at most 16 rows name the same one
- route_weight: float32 [256, 2], P('ep'), may hold values from 0.1 to 1
- expert_gate: bfloat16 [8, 4096, 2048], P('ep', None, 'tp'), may hold values from -0.25 to 0.25
- expert_up: bfloat16 [8, 4096, 2048], P('ep', None, 'tp'), may hold values from -0.25 to 0.25
- expert_down: bfloat16 [8, 2048, 4096], P('ep', 'tp'), may hold values from -0.03125 to 0.03125
Outputs:
- layer_out: bfloat16 [256, 4096], P('ep', 'tp')
- new_state: float32 [256, 8, 128, 128], P('ep', 'tp')
Inputs may be any that keep to these rules, and one draw needn't show every extreme that they name: `routing`: each row names 2 different experts. In each aligned block of 32 rows (the rows of one device) no expert is named more than 16 times, a bound that some block reaches.
All inputs are finite; a program needn't handle non-finite values.
Results may differ from a plain program's by a relative error of at most 0.019.
Values may be sent and summed in bfloat16 or wider, within the bound.
A program may use at most 64 MiB of HBM per device.

v0:
```python
import functools

import jax
import jax.numpy as jnp
from jax import lax
from jax.experimental import pallas as pl
from jax.experimental.pallas import tpu as pltpu
from jax.sharding import PartitionSpec as P

epsilon = 1e-06
clamp_limit = 7.0
swish_alpha = 1.702
MESH = pl.DeviceIdType.MESH
TOKEN_BLOCK = 8


def silu(values):
    return values * jax.nn.sigmoid(values)


def mix_kernel(
    tok_ref, gain_ref, dw_ref, sw_ref, rate_ref, hg_ref, wq_hbm, wk_hbm, wv_hbm, state_hbm,
    mixed_ref, new_hbm, wq_ref, wk_ref, wv_ref, state, q_scr, k_scr, v_scr, dec_scr, str_scr,
    ro_scr, w_sem, in_sem, out_sem,
):
    heads = state.shape[1]
    width = state.shape[2]
    block = TOKEN_BLOCK
    steps = state.shape[0] // block
    loads = []
    for i, (src, dst) in enumerate(((wq_hbm, wq_ref), (wk_hbm, wk_ref), (wv_hbm, wv_ref))):
        loads.append(pltpu.make_async_copy(src, dst, w_sem.at[i]))
        loads[-1].start()

    def take(i):
        rows = pl.ds(pl.multiple_of(i * block, block), block)
        return pltpu.make_async_copy(state_hbm.at[rows], state.at[rows], in_sem.at[i])

    def give(i):
        rows = pl.ds(pl.multiple_of(i * block, block), block)
        return pltpu.make_async_copy(state.at[rows], new_hbm.at[rows], out_sem.at[i])

    for i in range(steps):
        take(i).start()
    head_start = lax.axis_index("tp") * heads

    def first():
        values = tok_ref[...].astype(jnp.float32)
        scale = lax.rsqrt(jnp.mean(values * values, axis=-1, keepdims=True) + epsilon)
        normed = (values * scale * gain_ref[...].astype(jnp.float32)).astype(jnp.bfloat16)

        def project(i, w_ref):
            loads[i].wait()
            out = jnp.dot(normed, w_ref[...], preferred_element_type=jnp.float32)
            return silu(out.astype(jnp.bfloat16).astype(jnp.float32))

        dims = (((1,), (1,)), ((), ()))
        dec_pre = lax.dot_general(normed, dw_ref[...], dims, preferred_element_type=jnp.float32)
        str_pre = lax.dot_general(normed, sw_ref[...], dims, preferred_element_type=jnp.float32)
        cols = lax.broadcasted_iota(jnp.int32, dec_pre.shape, 1)
        queries, keys = project(0, wq_ref), project(1, wk_ref)
        v_scr[...] = project(2, wv_ref)
        for h in range(heads):
            part = slice(h * width, (h + 1) * width)
            q_h, k_h = queries[:, part], keys[:, part]
            q_scr[:, part] = q_h * lax.rsqrt(
                jnp.sum(q_h * q_h, axis=-1, keepdims=True) + epsilon
            ) * width ** (-0.5)
            k_scr[:, part] = k_h * lax.rsqrt(jnp.sum(k_h * k_h, axis=-1, keepdims=True) + epsilon)
            mine = cols == head_start + h
            d_h = jnp.sum(jnp.where(mine, dec_pre, 0.0), axis=1, keepdims=True)
            s_h = jnp.sum(jnp.where(mine, str_pre, 0.0), axis=1, keepdims=True)
            soft = jnp.maximum(d_h, 0.0) + jnp.log1p(jnp.exp(-jnp.abs(d_h)))
            decay = jnp.exp(-rate_ref[:, h:h + 1] * soft)
            dec_scr[:, part] = jnp.broadcast_to(decay, q_h.shape)
            str_scr[:, part] = jnp.broadcast_to(jax.nn.sigmoid(s_h), q_h.shape)

    first()

    def advance(step, carry):
        take(step).wait()
        rows = pl.ds(pl.multiple_of(step * block, block), block)
        for h in range(heads):
            part = slice(h * width, (h + 1) * width)
            q8, k8, v8 = q_scr[rows, part], k_scr[rows, part], v_scr[rows, part]
            d8, s8 = dec_scr[rows, part], str_scr[rows, part]
            qk8 = jnp.sum(q8 * k8, axis=1, keepdims=True)
            q_t, k_t = jnp.transpose(q8), jnp.transpose(k8)
            outs = []
            for t in range(block):
                memory = state[step * block + t, h]
                k_col, q_col = k_t[:, t:t + 1], q_t[:, t:t + 1]
                k_m = jnp.sum(memory * k_col, axis=0, keepdims=True)
                q_m = jnp.sum(memory * q_col, axis=0, keepdims=True)
                d_t = d8[t:t + 1]
                corrected = s8[t:t + 1] * (v8[t:t + 1] - d_t * k_m)
                state[step * block + t, h] = memory * d_t + k_col * corrected
                outs.append(d_t * q_m + qk8[t:t + 1] * corrected)
            ro_scr[rows, part] = jnp.concatenate(outs, axis=0)
        give(step).start()
        return carry

    lax.fori_loop(0, steps, advance, 0)

    gain = hg_ref[...].astype(jnp.float32)
    for h in range(heads):
        part = slice(h * width, (h + 1) * width)
        read = ro_scr[:, part]
        scale = lax.rsqrt(jnp.mean(read * read, axis=-1, keepdims=True) + epsilon)
        mixed_ref[:, part] = (read * scale * gain).astype(jnp.bfloat16)
    for i in range(steps):
        give(i).wait()


def mix_step(tokens, mix_gain, wq, wk, wv, dw, sw, rate, head_gain, state):
    rows, _ = tokens.shape
    heads, width = state.shape[1], state.shape[2]
    inner = heads * width
    vmem = pl.BlockSpec(memory_space=pltpu.VMEM)
    hbm = pl.BlockSpec(memory_space=pl.ANY)
    sem = pltpu.SemaphoreType.DMA
    steps = rows // TOKEN_BLOCK
    return pl.pallas_call(
        mix_kernel,
        out_shape=(
            jax.ShapeDtypeStruct((rows, inner), jnp.bfloat16),
            jax.ShapeDtypeStruct(state.shape, state.dtype),
        ),
        in_specs=[vmem] * 6 + [hbm] * 4,
        out_specs=(vmem, hbm),
        scratch_shapes=[pltpu.VMEM(w.shape, w.dtype) for w in (wq, wk, wv, state)]
        + [pltpu.VMEM((rows, inner), jnp.float32)] * 6
        + [sem((3,)), sem((steps,)), sem((steps,))],
        compiler_params=pltpu.CompilerParams(vmem_limit_bytes=62 * 1024 * 1024),
        name="mix",
    )(tokens, mix_gain, dw, sw, rate, head_gain, wq, wk, wv, state)


def expert_kernel(
    groups, tp_width, capacity,
    tok_ref, mixed_ref, gain_ref, route_ref, weight_ref, wo_hbm, wg_hbm, wu_hbm, wd_hbm,
    out_ref,
    wo, wg, wu, wd, part, rs_in, ss_out, ss_in, out_buf, x_buf, po, pair_in, pair_sum, y_in,
    ret_out, ret_in, res_scr, gate_acc, up_acc,
    load_sem, rs_s, rs_r, ss_s, ss_r, a2a_s, a2a_r, agy_s, agy_r, agp_s, agp_r,
    pr_s, pr_r, yr_s, yr_r, rt_s, rt_r,
):
    ep, tp = lax.axis_index("ep"), lax.axis_index("tp")
    rows, model = tok_ref.shape
    share = model // tp_width
    chips = tp_width // 2
    slots = groups * capacity
    chip, core = tp // 2, lax.rem(tp, 2)
    partner = chip * 2 + 1 - core

    loads = []
    for i, (src, dst) in enumerate(((wo_hbm, wo), (wg_hbm, wg), (wu_hbm, wu), (wd_hbm, wd))):
        loads.append(pltpu.make_async_copy(src, dst, load_sem.at[i]))
        loads[-1].start()

    barrier = pltpu.get_barrier_semaphore()
    for k in range(1, tp_width):
        pl.semaphore_signal(
            barrier, inc=1, device_id=(ep, lax.rem(tp + k, tp_width)), device_id_type=MESH
        )
    for k in range(1, groups):
        pl.semaphore_signal(
            barrier, inc=1, device_id=(lax.rem(ep + k, groups), tp), device_id_type=MESH
        )

    sends = []

    def send(src, dst, s_sem, r_sem, target):
        copy = pltpu.make_async_remote_copy(
            src_ref=src, dst_ref=dst, send_sem=s_sem, recv_sem=r_sem,
            device_id=target, device_id_type=MESH,
        )
        copy.start()
        sends.append(copy)

    def arrive(ref, r_sem, s_sem):
        pltpu.make_async_remote_copy(
            src_ref=ref, dst_ref=ref, send_sem=s_sem, recv_sem=r_sem,
            device_id=(ep, partner), device_id_type=MESH,
        ).wait_recv()

    top = route_ref.shape[1]
    slot_ids = lax.broadcasted_iota(jnp.int32, (rows, slots), 1)
    slot_expert = slot_ids // capacity
    slot_rank = slot_ids % capacity
    marks = [route_ref[:, k:k + 1] == slot_expert for k in range(top)]
    named = functools.reduce(lambda a, b: a + b, [m.astype(jnp.float32) for m in marks])
    before = (
        lax.broadcasted_iota(jnp.int32, (rows, rows), 0)
        > lax.broadcasted_iota(jnp.int32, (rows, rows), 1)
    ).astype(jnp.float32).astype(jnp.bfloat16)
    ranks = jnp.dot(before, named.astype(jnp.bfloat16), preferred_element_type=jnp.float32)
    here = ranks == slot_rank.astype(jnp.float32)
    chosen = [jnp.where(jnp.logical_and(m, here), 1.0, 0.0) for m in marks]
    place = functools.reduce(lambda a, b: a + b, chosen).astype(jnp.bfloat16)
    blend = functools.reduce(
        lambda a, b: a + b, [c * weight_ref[:, k:k + 1] for k, c in enumerate(chosen)]
    )

    loads[0].wait()
    for p in range(tp_width):
        part[p] = jnp.dot(
            mixed_ref[...], wo[:, p * share:(p + 1) * share], preferred_element_type=jnp.float32
        ).astype(jnp.bfloat16)
    pl.semaphore_wait(barrier, tp_width - 1 + groups - 1)
    for k in range(1, tp_width):
        to = lax.rem(tp + k, tp_width)
        send(part.at[to], rs_in.at[k], rs_s.at[k], rs_r.at[k], (ep, to))
    total = part[tp].astype(jnp.float32)
    for k in range(1, tp_width):
        arrive(rs_in.at[k], rs_r.at[k], rs_s.at[k])
        total = total + rs_in[k].astype(jnp.float32)
    cols = pl.ds(pl.multiple_of(tp * share, share), share)
    residual = (tok_ref[:, cols].astype(jnp.float32) + total).astype(jnp.bfloat16)
    res_scr[...] = residual
    res = residual.astype(jnp.float32)
    squares = jnp.sum(res * res, axis=-1, keepdims=True)
    ss_out[...] = jnp.broadcast_to(squares, ss_out.shape)
    for k in range(1, tp_width):
        to = lax.rem(tp + k, tp_width)
        send(ss_out, ss_in.at[k], ss_s.at[k], ss_r.at[k], (ep, to))
    for k in range(1, tp_width):
        arrive(ss_in.at[k], ss_r.at[k], ss_s.at[k])
        squares = squares + ss_in[k][:, 0:1]
    scale = lax.rsqrt(squares / model + epsilon)
    ffn = (res * scale * gain_ref[:, cols].astype(jnp.float32)).astype(jnp.bfloat16)

    outgoing = lax.dot_general(
        place, ffn, (((0,), (0,)), ((), ())), preferred_element_type=jnp.float32
    ).astype(jnp.bfloat16)
    out_buf[...] = outgoing.reshape(groups, capacity, share)
    for k in range(1, groups):
        to = lax.rem(ep + k, groups)
        send(out_buf.at[to], x_buf.at[tp, ep], a2a_s.at[k], a2a_r.at[k], (to, tp))
    x_buf[tp, ep] = out_buf[ep]

    for k in range(groups):
        src = lax.rem(ep + groups - k, groups)
        block = x_buf.at[tp, src]
        if k > 0:
            arrive(block, a2a_r.at[k], a2a_s.at[k])
        for c in range(1, chips):
            to = lax.rem(chip + c, chips) * 2 + core
            send(block, block, agy_s.at[c, k], agy_r.at[c, k], (ep, to))
        send(block, block, agp_s.at[0, k], agp_r.at[0, k], (ep, partner))

    loads[1].wait()
    loads[2].wait()

    def accumulate(j, first):
        x = x_buf[j].reshape(slots, share)
        depth = pl.ds(pl.multiple_of(j * share, share), share)
        g = jnp.dot(x, wg[depth, :], preferred_element_type=jnp.float32)
        u = jnp.dot(x, wu[depth, :], preferred_element_type=jnp.float32)
        gate_acc[...] = g if first else gate_acc[...] + g
        up_acc[...] = u if first else up_acc[...] + u

    accumulate(tp, True)
    for c in range(1, chips):
        origin = lax.rem(chip + chips - c, chips) * 2 + core
        for k in range(groups):
            src = lax.rem(ep + groups - k, groups)
            block = x_buf.at[origin, src]
            arrive(block, agy_r.at[c, k], agy_s.at[c, k])
            send(block, block, agp_s.at[c, k], agp_r.at[c, k], (ep, partner))
    for k in range(groups):
        src = lax.rem(ep + groups - k, groups)
        arrive(x_buf.at[partner, src], agp_r.at[0, k], agp_s.at[0, k])
    accumulate(partner, False)
    for c in range(1, chips):
        other = lax.rem(chip + chips - c, chips) * 2
        accumulate(other + core, False)
        for k in range(groups):
            src = lax.rem(ep + groups - k, groups)
            arrive(x_buf.at[other + 1 - core, src], agp_r.at[c, k], agp_s.at[c, k])
        accumulate(other + 1 - core, False)

    gate_cut = jnp.minimum(gate_acc[...], clamp_limit)
    up_cut = jnp.clip(up_acc[...], -clamp_limit, clamp_limit)
    hidden = ((up_cut + 1.0) * gate_cut * jax.nn.sigmoid(swish_alpha * gate_cut)).astype(
        jnp.bfloat16
    )

    loads[3].wait()

    def down(p):
        lanes = pl.ds(pl.multiple_of(p * share, share), share)
        term = jnp.dot(hidden, wd[:, lanes], preferred_element_type=jnp.float32)
        po[p] = term.astype(jnp.bfloat16).reshape(groups, capacity, share)

    order = [lax.rem(chip + c, chips) for c in list(range(1, chips)) + [0]]
    for i, c in enumerate(order):
        down(c * 2 + 1 - core)
        send(po.at[c * 2 + 1 - core], pair_in.at[i], pr_s.at[i], pr_r.at[i], (ep, partner))
        if i < chips - 1:
            down(c * 2 + core)
    for i, c in enumerate(order[:-1]):
        arrive(pair_in.at[i], pr_r.at[i], pr_s.at[i])
        for k in list(range(1, groups)) + [0]:
            s = lax.rem(ep + k, groups)
            pair_sum[i, s] = (
                po[c * 2 + core, s].astype(jnp.float32) + pair_in[i, s].astype(jnp.float32)
            ).astype(jnp.bfloat16)
            send(
                pair_sum.at[i, s], y_in.at[i, s], yr_s.at[i, k], yr_r.at[i, k],
                (ep, c * 2 + core),
            )
    last = chips - 1
    down(tp)
    arrive(pair_in.at[last], pr_r.at[last], pr_s.at[last])
    for k in list(range(1, groups)) + [0]:
        s = lax.rem(ep + k, groups)
        term = po[tp, s].astype(jnp.float32) + pair_in[last, s].astype(jnp.float32)
        for i in range(chips - 1):
            arrive(y_in.at[i, s], yr_r.at[i, k], yr_s.at[i, k])
            term = term + y_in[i, s].astype(jnp.float32)
        if k > 0:
            ret_out[s] = term.astype(jnp.bfloat16)
            send(ret_out.at[s], ret_in.at[ep], rt_s.at[k], rt_r.at[k], (s, tp))
        else:
            ret_in[s] = term.astype(jnp.bfloat16)
    for k in range(1, groups):
        src = lax.rem(ep + groups - k, groups)
        arrive(ret_in.at[src], rt_r.at[k], rt_s.at[k])

    back = ret_in[...].reshape(slots, share)
    high = blend.astype(jnp.bfloat16)
    low = (blend - high.astype(jnp.float32)).astype(jnp.bfloat16)
    routed = jnp.dot(high, back, preferred_element_type=jnp.float32) + jnp.dot(
        low, back, preferred_element_type=jnp.float32
    )
    out_ref[...] = (res_scr[...].astype(jnp.float32) + routed).astype(jnp.bfloat16)
    for copy in sends:
        copy.wait_send()


def expert_step(tokens, mixed, gain, routing, route_weight, wo, wg, wu, wd):
    groups, tp_width = lax.axis_size("ep"), lax.axis_size("tp")
    rows, model = tokens.shape
    share = model // tp_width
    chips = tp_width // 2
    need = 2 * rows * routing.shape[1] // groups
    capacity = -(-need // 16) * 16
    slots = groups * capacity
    ff = wg.shape[1]
    bf16, f32 = jnp.bfloat16, jnp.float32
    vmem = pl.BlockSpec(memory_space=pltpu.VMEM)
    hbm = pl.BlockSpec(memory_space=pl.ANY)
    block = (groups, capacity, share)
    sem = pltpu.SemaphoreType.DMA
    return pl.pallas_call(
        functools.partial(expert_kernel, groups, tp_width, capacity),
        out_shape=jax.ShapeDtypeStruct((rows, share), bf16),
        in_specs=[vmem] * 5 + [hbm] * 4,
        out_specs=vmem,
        scratch_shapes=[
            pltpu.VMEM(wo.shape, bf16), pltpu.VMEM(wg.shape, bf16),
            pltpu.VMEM(wu.shape, bf16), pltpu.VMEM(wd.shape, bf16),
            pltpu.VMEM((tp_width, rows, share), bf16),
            pltpu.VMEM((tp_width, rows, share), bf16),
            pltpu.VMEM((rows, 128), f32),
            pltpu.VMEM((tp_width, rows, 128), f32),
            pltpu.VMEM(block, bf16),
            pltpu.VMEM((tp_width,) + block, bf16),
            pltpu.VMEM((tp_width,) + block, bf16),
            pltpu.VMEM((chips,) + block, bf16),
            pltpu.VMEM((chips,) + block, bf16),
            pltpu.VMEM((chips,) + block, bf16),
            pltpu.VMEM(block, bf16),
            pltpu.VMEM(block, bf16),
            pltpu.VMEM((rows, share), bf16),
            pltpu.VMEM((slots, ff), f32),
            pltpu.VMEM((slots, ff), f32),
            sem((4,)),
            sem((tp_width,)), sem((tp_width,)),
            sem((tp_width,)), sem((tp_width,)),
            sem((groups,)), sem((groups,)),
            sem((chips, groups)), sem((chips, groups)),
            sem((chips, groups)), sem((chips, groups)),
            sem((chips,)), sem((chips,)),
            sem((chips, groups)), sem((chips, groups)),
            sem((groups,)), sem((groups,)),
        ],
        compiler_params=pltpu.CompilerParams(
            collective_id=0, has_side_effects=True, vmem_limit_bytes=62 * 1024 * 1024
        ),
        name="experts",
    )(tokens, mixed, gain, routing, route_weight, wo, wg, wu, wd)


def on_device(
    tokens,
    mix_gain,
    query_weight,
    key_weight,
    value_weight,
    decay_weight,
    strength_weight,
    decay_rate,
    head_gain,
    memory_state,
    output_weight,
    ffn_gain,
    routing,
    route_weight,
    expert_gate,
    expert_up,
    expert_down,
):
    mixed, new_state = mix_step(
        tokens, mix_gain[None, :], query_weight, key_weight, value_weight,
        decay_weight.T, strength_weight.T, decay_rate[None, :], head_gain[None, :], memory_state,
    )
    layer_out = expert_step(
        tokens, mixed, ffn_gain[None, :], routing, route_weight, output_weight,
        expert_gate[0], expert_up[0], expert_down[0],
    )
    return (layer_out, new_state)


def solution(mesh):
    placed = (
        P("ep", None),
        P(),
        P(None, "tp"),
        P(None, "tp"),
        P(None, "tp"),
        P(),
        P(),
        P("tp"),
        P(),
        P("ep", "tp", None, None),
        P("tp", None),
        P(),
        P("ep", None),
        P("ep", None),
        P("ep", None, "tp"),
        P("ep", None, "tp"),
        P("ep", "tp", None),
    )
    return jax.shard_map(
        on_device,
        mesh=mesh,
        in_specs=placed,
        out_specs=(P("ep", "tp"), P("ep", "tp", None, None)),
        check_vma=False,
    )
```

profile of v0, /device:TPU:0, one launch (start us, length us, event | category | flops | bytes accessed | tf_op | source)
XLA Modules:
  0.0 58.0 jit_solution(15954724480779287169)
XLA Ops:
  0.6 1.3 %broadcast_in_dim.12.gain_ref = bf16[1,4096]{1,0:T(2,128)(2,1)} reshape(bf16[4096]{0:T(1024)(128)(2,1)} %param.18) | data formatting | bytes 16384 | tf_op jit(solution)/shard_map/broadcast_in_dim | solution.py:416
  1.9 1.3 %broadcast_in_dim.15.gain_ref = bf16[1,4096]{1,0:T(2,128)(2,1)} reshape(bf16[4096]{0:T(1024)(128)(2,1)} %param.28) | data formatting | bytes 16384 | tf_op jit(solution)/shard_map/broadcast_in_dim | solution.py:420
  3.2 1.4 %copy.19.route_ref = s32[32,2]{1,0:T(8,128)} copy(s32[32,2]{0,1:T(2,128)} %param.29) | data formatting | bytes 512 | tf_op args[12]
  4.6 1.4 %copy.20.weight_ref = f32[32,2]{1,0:T(8,128)} copy(f32[32,2]{0,1:T(2,128)} %param.30) | data formatting | bytes 512 | tf_op args[13]
  6.0 10.6 %mix.1 = (bf16[32,256]{1,0:T(8,128)(2,1)}, f32[32,2,128,128]{3,2,1,0:T(8,128)}) custom-call(bf16[32,4096]{1,0:T(8,128)(2,1)} %tok_ref.3, bf16[1,4096]{1,0:T(2,128)(2,1)} %broadcast_in_dim.12.gain_ref, bf16[8,4096]{1,0:T(8,128)(2,1)} %bitcast.10, bf16[8,4096]{1,0:T(8,128)(2,1)} %bitcast.11, f32[1,2]{1,0:T(1,128)} %bitcast.12, bf16[1,128]{1,0:T(2,128)(2,1)} %bitcast.13, ...), custom_call_target="tpu_custom_call" | custom-call | tf_op jit(solution)/shard_map/mix/pallas_call | solution.py:123
  16.6 40.0 %experts.1 = bf16[32,1024]{1,0:T(8,128)(2,1)} custom-call(bf16[32,4096]{1,0:T(8,128)(2,1)} %tok_ref.3, bf16[32,256]{1,0:T(8,128)(2,1)} %get-tuple-element.4.mixed_ref, bf16[1,4096]{1,0:T(2,128)(2,1)} %broadcast_in_dim.15.gain_ref, s32[32,2]{1,0:T(8,128)} %copy.19.route_ref, f32[32,2]{1,0:T(8,128)} %copy.20.weight_ref, bf16[256,4096]{1,0:T(8,128)(2,1)} %wo_hbm.1, ...), custom_call_target="tpu_custom_call" | custom-call | tf_op jit(solution)/shard_map/experts/pallas_call | solution.py:356
  56.6 1.5 %copy.22 = bf16[32,1024]{1,0:T(8,128)(2,1)} copy(bf16[32,1024]{1,0:T(8,128)(2,1)} %experts.1) | data formatting | bytes 131072
where the time goes:
time: 58.4 us; the launch traced here: 58 us
  Pallas kernels  50.6 us (87%)
  local copies, waits for them, and re-layouts  6.8 us (12%)
  between operations  0.65 us (1%)
    pallas_call x1, Pallas kernels, expert_step(): pl.pallas_call(functools.partial(expert_kernel, groups, tp_width, capacit...  40 us
    pallas_call x1, Pallas kernels, mix_step(): pl.pallas_call(mix_kernel, out_shape=(jax.ShapeDtypeStruct((rows, inner),...  10.6 us
    unnamed x3, local copies, waits for them, and re-layouts  4.19 us
    broadcast_in_dim x1, local copies, waits for them, and re-layouts, on_device(): mix_gain[None, :]  1.31 us
    broadcast_in_dim x1, local copies, waits for them, and re-layouts, on_device(): ffn_gain[None, :]  1.3 us

commit v1 on v0

v1 whole, which is shorter than its diff:
```python
import functools

import jax
import jax.numpy as jnp
from jax import lax
from jax.experimental import pallas as pl
from jax.experimental.pallas import tpu as pltpu
from jax.sharding import PartitionSpec as P

epsilon = 1e-06
clamp_limit = 7.0
swish_alpha = 1.702
MESH = pl.DeviceIdType.MESH
TOKEN_BLOCK = 8
MIX_VMEM = 20 * 1024 * 1024
EXPERT_VMEM = 32 * 1024 * 1024


def silu(values):
    return values * jax.nn.sigmoid(values)


def mix_kernel(
    tok_hbm, gain_hbm, dw_hbm, sw_hbm, rate_hbm, hg_hbm, wq_hbm, wk_hbm, wv_hbm, state_hbm,
    mixed_ref, new_hbm, tok_ref, gain_ref, dw_ref, sw_ref, rate_ref, hg_ref, wq_ref, wk_ref,
    wv_ref, state, q_scr, k_scr, v_scr, dec_scr, str_scr, ro_scr, l_sem, in_sem, out_sem,
):
    heads = state.shape[1]
    width = state.shape[2]
    block = TOKEN_BLOCK
    steps = state.shape[0] // block
    loads = []
    for i, (src, dst) in enumerate((
        (tok_hbm, tok_ref), (gain_hbm, gain_ref), (wq_hbm, wq_ref), (dw_hbm, dw_ref),
        (sw_hbm, sw_ref), (rate_hbm, rate_ref), (hg_hbm, hg_ref), (wk_hbm, wk_ref),
        (wv_hbm, wv_ref),
    )):
        loads.append(pltpu.make_async_copy(src, dst, l_sem.at[i]))
        loads[-1].start()
    tok_in, gain_in, wq_in, dw_in, sw_in, rate_in, hg_in, wk_in, wv_in = loads

    def take(i):
        rows = pl.ds(pl.multiple_of(i * block, block), block)
        return pltpu.make_async_copy(state_hbm.at[rows], state.at[rows], in_sem.at[i])

    def give(i):
        rows = pl.ds(pl.multiple_of(i * block, block), block)
        return pltpu.make_async_copy(state.at[rows], new_hbm.at[rows], out_sem.at[i])

    for i in range(steps):
        take(i).start()
    head_start = lax.axis_index("tp") * heads

    tok_in.wait()
    gain_in.wait()
    values = tok_ref[...].astype(jnp.float32)
    scale = lax.rsqrt(jnp.mean(values * values, axis=-1, keepdims=True) + epsilon)
    gain = gain_ref[...].astype(jnp.float32)
    lanes = gain.shape[1]
    normed = jnp.concatenate(
        [
            (values[:, i * lanes:(i + 1) * lanes] * scale * gain[i:i + 1]).astype(jnp.bfloat16)
            for i in range(gain.shape[0])
        ],
        axis=1,
    )

    def project(copy, w_ref):
        copy.wait()
        out = jnp.dot(normed, w_ref[...], preferred_element_type=jnp.float32)
        return silu(out.astype(jnp.bfloat16).astype(jnp.float32))

    dw_in.wait()
    sw_in.wait()
    rate_in.wait()
    wide = normed.astype(jnp.float32)

    def per_head(w_ref, h):
        w = w_ref[...].astype(jnp.float32)
        mine = lax.broadcasted_iota(jnp.int32, w.shape, 0) == head_start + h
        row = jnp.sum(jnp.where(mine, w, 0.0), axis=0, keepdims=True)
        return jnp.sum(wide * row, axis=1, keepdims=True)

    for h in range(heads):
        part = slice(h * width, (h + 1) * width)
        d_h, s_h = per_head(dw_ref, h), per_head(sw_ref, h)
        soft = jnp.maximum(d_h, 0.0) + jnp.log1p(jnp.exp(-jnp.abs(d_h)))
        decay = jnp.exp(-rate_ref[:, h:h + 1] * soft)
        spread = (d_h.shape[0], width)
        dec_scr[:, part] = jnp.broadcast_to(decay, spread)
        str_scr[:, part] = jnp.broadcast_to(jax.nn.sigmoid(s_h), spread)

    def unit(values):
        return values * lax.rsqrt(jnp.sum(values * values, axis=-1, keepdims=True) + epsilon)

    queries = project(wq_in, wq_ref)
    for h in range(heads):
        part = slice(h * width, (h + 1) * width)
        q_scr[:, part] = unit(queries[:, part]) * width ** (-0.5)
    keys = project(wk_in, wk_ref)
    for h in range(heads):
        part = slice(h * width, (h + 1) * width)
        k_scr[:, part] = unit(keys[:, part])
    v_scr[...] = project(wv_in, wv_ref)

    def advance(step, carry):
        take(step).wait()
        rows = pl.ds(pl.multiple_of(step * block, block), block)
        for h in range(heads):
            part = slice(h * width, (h + 1) * width)
            q8, k8, v8 = q_scr[rows, part], k_scr[rows, part], v_scr[rows, part]
            d8, s8 = dec_scr[rows, part], str_scr[rows, part]
            qk8 = jnp.sum(q8 * k8, axis=1, keepdims=True)
            q_t, k_t = jnp.transpose(q8), jnp.transpose(k8)
            outs = []
            for t in range(block):
                memory = state[step * block + t, h]
                k_col, q_col = k_t[:, t:t + 1], q_t[:, t:t + 1]
                k_m = jnp.sum(memory * k_col, axis=0, keepdims=True)
                q_m = jnp.sum(memory * q_col, axis=0, keepdims=True)
                d_t = d8[t:t + 1]
                corrected = s8[t:t + 1] * (v8[t:t + 1] - d_t * k_m)
                state[step * block + t, h] = memory * d_t + k_col * corrected
                outs.append(d_t * q_m + qk8[t:t + 1] * corrected)
            ro_scr[rows, part] = jnp.concatenate(outs, axis=0)
        give(step).start()
        return carry

    lax.fori_loop(0, steps, advance, 0)

    hg_in.wait()
    head_gain = hg_ref[...].astype(jnp.float32)
    for h in range(heads):
        part = slice(h * width, (h + 1) * width)
        read = ro_scr[:, part]
        scale = lax.rsqrt(jnp.mean(read * read, axis=-1, keepdims=True) + epsilon)
        mixed_ref[:, part] = (read * scale * head_gain).astype(jnp.bfloat16)
    for i in range(steps):
        give(i).wait()


def mix_step(tokens, mix_gain, wq, wk, wv, dw, sw, rate, head_gain, state):
    rows, _ = tokens.shape
    heads, width = state.shape[1], state.shape[2]
    inner = heads * width
    hbm = pl.BlockSpec(memory_space=pltpu.HBM)
    sem = pltpu.SemaphoreType.DMA
    steps = rows // TOKEN_BLOCK
    args = [
        pltpu.with_memory_space_constraint(a, pltpu.HBM) if a.size > 1 else a
        for a in (tokens, mix_gain, dw, sw, rate, head_gain, wq, wk, wv, state)
    ]
    return pl.pallas_call(
        mix_kernel,
        out_shape=(
            jax.ShapeDtypeStruct((rows, inner), jnp.bfloat16),
            jax.ShapeDtypeStruct(state.shape, state.dtype),
        ),
        in_specs=[hbm] * 10,
        out_specs=(pl.BlockSpec(memory_space=pltpu.VMEM), hbm),
        scratch_shapes=[pltpu.VMEM(a.shape, a.dtype) for a in args]
        + [pltpu.VMEM((rows, inner), jnp.float32)] * 6
        + [sem((9,)), sem((steps,)), sem((steps,))],
        compiler_params=pltpu.CompilerParams(vmem_limit_bytes=MIX_VMEM),
        name="mix",
    )(*args)


def expert_kernel(
    groups, tp_width, capacity,
    mixed_ref, tok_ref, gain_ref, route_ref, weight_ref, wo, wg_hbm, wu_hbm, wd_hbm,
    out_ref,
    wg, wu, wd, gain_scr,
    part, rs_in, ss_out, ss_in, sc_out, sc_in, out_buf, x_buf, po, pair_in, pair_sum, y_in,
    ret_out, ret_in, res_scr, gate_acc, up_acc,
    load_sem, rs_s, rs_r, ss_s, ss_r, sc_s, sc_r, a2a_s, a2a_r, agy_s, agy_r, agp_s, agp_r,
    pr_s, pr_r, yr_s, yr_r, rt_s, rt_r,
):
    ep, tp = lax.axis_index("ep"), lax.axis_index("tp")
    rows, model = tok_ref.shape
    share = model // tp_width
    chips = tp_width // 2
    slots = groups * capacity
    chip, core = tp // 2, lax.rem(tp, 2)
    partner = chip * 2 + 1 - core
    cols = pl.ds(pl.multiple_of(tp * share, share), share)

    loads = [
        pltpu.make_async_copy(src, dst, load_sem.at[i])
        for i, (src, dst) in enumerate(((wg_hbm, wg), (wu_hbm, wu), (wd_hbm, wd)))
    ]
    wg_in, wu_in, wd_in = loads
    for copy in loads:
        copy.start()

    barrier = pltpu.get_barrier_semaphore()
    for k in range(1, groups):
        pl.semaphore_signal(
            barrier, inc=1, device_id=(lax.rem(ep + k, groups), tp), device_id_type=MESH
        )
    for k in range(1, tp_width):
        pl.semaphore_signal(
            barrier, inc=1, device_id=(ep, lax.rem(tp + k, tp_width)), device_id_type=MESH
        )

    sends = []

    def send(src, dst, s_sem, r_sem, target):
        copy = pltpu.make_async_remote_copy(
            src_ref=src, dst_ref=dst, send_sem=s_sem, recv_sem=r_sem,
            device_id=target, device_id_type=MESH,
        )
        copy.start()
        sends.append(copy)

    def arrive(ref, r_sem, s_sem):
        pltpu.make_async_remote_copy(
            src_ref=ref, dst_ref=ref, send_sem=s_sem, recv_sem=r_sem,
            device_id=(ep, partner), device_id_type=MESH,
        ).wait_recv()

    peers = []
    for c in list(range(1, chips)) + [0]:
        for b in (0, 1):
            if c or b:
                at = lax.rem(chip + c, chips) * 2
                peers.append((c * 2 + b, at + (1 - core if b else core)))

    def project(p):
        lanes = pl.ds(pl.multiple_of(p * share, share), share)
        part[p] = jnp.dot(
            mixed_ref[...], wo[:, lanes], preferred_element_type=jnp.float32
        ).astype(jnp.bfloat16)

    for _, to in peers[:-1]:
        project(to)
    pl.semaphore_wait(barrier, tp_width - 1 + groups - 1)
    for j, to in peers:
        if j == 1:
            project(to)
        send(part.at[to], rs_in.at[j], rs_s.at[j], rs_r.at[j], (ep, to))
    project(tp)

    top = route_ref.shape[0]
    slot_ids = lax.broadcasted_iota(jnp.int32, (slots, rows), 0)
    slot_expert = slot_ids // capacity
    slot_rank = slot_ids % capacity
    marks = [route_ref[k:k + 1, :] == slot_expert for k in range(top)]
    named = functools.reduce(lambda a, b: a + b, [m.astype(jnp.float32) for m in marks])
    before = (
        lax.broadcasted_iota(jnp.int32, (rows, rows), 0)
        < lax.broadcasted_iota(jnp.int32, (rows, rows), 1)
    ).astype(jnp.float32).astype(jnp.bfloat16)
    ranks = jnp.dot(named.astype(jnp.bfloat16), before, preferred_element_type=jnp.float32)
    here = ranks == slot_rank.astype(jnp.float32)
    chosen = [jnp.where(jnp.logical_and(m, here), 1.0, 0.0) for m in marks]
    place = functools.reduce(lambda a, b: a + b, chosen)
    place_t = jnp.transpose(place)
    place = place.astype(jnp.bfloat16)
    blend = functools.reduce(
        lambda a, b: a + b, [c * weight_ref[k:k + 1, :] for k, c in enumerate(chosen)]
    )
    gain_scr[...] = gain_ref[...].astype(jnp.float32)
    diag = (
        lax.broadcasted_iota(jnp.int32, (rows, 128), 0)
        == lax.broadcasted_iota(jnp.int32, (rows, 128), 1)
    )

    total = tok_ref[:, cols].astype(jnp.float32)
    mix_sum = part[tp].astype(jnp.float32)
    for j, _ in reversed(peers):
        arrive(rs_in.at[j], rs_r.at[j], rs_s.at[j])
        mix_sum = mix_sum + rs_in[j].astype(jnp.float32)
    residual = (total + mix_sum).astype(jnp.bfloat16)
    res_scr[...] = residual
    res = residual.astype(jnp.float32)
    blocks = share // 128
    scaled = jnp.concatenate(
        [
            (
                res[:, i * 128:(i + 1) * 128] * gain_scr[pl.ds(tp * blocks + i, 1), :]
            ).astype(jnp.bfloat16)
            for i in range(blocks)
        ],
        axis=1,
    )
    outgoing = jnp.dot(place, scaled, preferred_element_type=jnp.float32).astype(jnp.bfloat16)
    out_buf[...] = outgoing.reshape(groups, capacity, share)
    for k in range(1, groups):
        to = lax.rem(ep + k, groups)
        send(out_buf.at[to], x_buf.at[tp, ep], a2a_s.at[k], a2a_r.at[k], (to, tp))
    x_buf[tp, ep] = out_buf[ep]

    squares = jnp.sum(res * res, axis=-1, keepdims=True)
    ss_out[...] = jnp.sum(jnp.where(diag, squares, 0.0), axis=0, keepdims=True)
    for j, to in peers:
        send(ss_out, ss_in.at[j], ss_s.at[j], ss_r.at[j], (ep, to))

    for k in range(groups):
        src = lax.rem(ep + groups - k, groups)
        block = x_buf.at[tp, src]
        if k > 0:
            arrive(block, a2a_r.at[k], a2a_s.at[k])
        for c in range(1, chips):
            to = lax.rem(chip + c, chips) * 2 + core
            send(block, block, agy_s.at[c, k], agy_r.at[c, k], (ep, to))
        send(block, block, agp_s.at[0, k], agp_r.at[0, k], (ep, partner))

    sum_row = ss_out[...]
    for j, _ in peers:
        arrive(ss_in.at[j], ss_r.at[j], ss_s.at[j])
        sum_row = sum_row + ss_in[j]
    scale_row = lax.rsqrt(sum_row / model + epsilon)
    scale = jnp.sum(jnp.where(diag, scale_row, 0.0), axis=1, keepdims=True)
    slot_scale = jnp.sum(place_t * scale, axis=0, keepdims=True)
    sc_out[...] = slot_scale
    for k in range(1, groups):
        to = lax.rem(ep + k, groups)
        send(sc_out, sc_in.at[ep], sc_s.at[k], sc_r.at[k], (to, tp))
    sc_in[ep] = slot_scale

    wg_in.wait()
    wu_in.wait()

    def accumulate(j, first):
        x = x_buf[j].reshape(slots, share)
        depth = pl.ds(pl.multiple_of(j * share, share), share)
        g = jnp.dot(x, wg[depth, :], preferred_element_type=jnp.float32)
        u = jnp.dot(x, wu[depth, :], preferred_element_type=jnp.float32)
        gate_acc[...] = g if first else gate_acc[...] + g
        up_acc[...] = u if first else up_acc[...] + u

    accumulate(tp, True)
    for c in range(1, chips):
        origin = lax.rem(chip + chips - c, chips) * 2 + core
        for k in range(groups):
            src = lax.rem(ep + groups - k, groups)
            block = x_buf.at[origin, src]
            arrive(block, agy_r.at[c, k], agy_s.at[c, k])
            send(block, block, agp_s.at[c, k], agp_r.at[c, k], (ep, partner))
    for k in range(groups):
        src = lax.rem(ep + groups - k, groups)
        arrive(x_buf.at[partner, src], agp_r.at[0, k], agp_s.at[0, k])
    accumulate(partner, False)
    for c in range(1, chips):
        other = lax.rem(chip + chips - c, chips) * 2
        accumulate(other + core, False)
        for k in range(groups):
            src = lax.rem(ep + groups - k, groups)
            arrive(x_buf.at[other + 1 - core, src], agp_r.at[c, k], agp_s.at[c, k])
        accumulate(other + 1 - core, False)

    for k in range(1, groups):
        src = lax.rem(ep + groups - k, groups)
        arrive(sc_in.at[src], sc_r.at[k], sc_s.at[k])
    picks = (
        lax.broadcasted_iota(jnp.int32, (capacity, slots), 1)
        == lax.broadcasted_iota(jnp.int32, (capacity, slots), 0) + ep * capacity
    )
    row_scale = jnp.concatenate(
        [
            jnp.sum(jnp.where(picks, sc_in[s], 0.0), axis=1, keepdims=True)
            for s in range(groups)
        ],
        axis=0,
    )
    gate_cut = jnp.minimum(gate_acc[...] * row_scale, clamp_limit)
    up_cut = jnp.clip(up_acc[...] * row_scale, -clamp_limit, clamp_limit)
    hidden = ((up_cut + 1.0) * gate_cut * jax.nn.sigmoid(swish_alpha * gate_cut)).astype(
        jnp.bfloat16
    )

    wd_in.wait()

    def down(p):
        lanes = pl.ds(pl.multiple_of(p * share, share), share)
        term = jnp.dot(hidden, wd[:, lanes], preferred_element_type=jnp.float32)
        po[p] = term.astype(jnp.bfloat16).reshape(groups, capacity, share)

    order = [lax.rem(chip + c, chips) for c in list(range(1, chips)) + [0]]
    for i, c in enumerate(order):
        down(c * 2 + 1 - core)
        send(po.at[c * 2 + 1 - core], pair_in.at[i], pr_s.at[i], pr_r.at[i], (ep, partner))
        if i < chips - 1:
            down(c * 2 + core)
    for i, c in enumerate(order[:-1]):
        arrive(pair_in.at[i], pr_r.at[i], pr_s.at[i])
        for k in list(range(1, groups)) + [0]:
            s = lax.rem(ep + k, groups)
            pair_sum[i, s] = (
                po[c * 2 + core, s].astype(jnp.float32) + pair_in[i, s].astype(jnp.float32)
            ).astype(jnp.bfloat16)
            send(
                pair_sum.at[i, s], y_in.at[i, s], yr_s.at[i, k], yr_r.at[i, k],
                (ep, c * 2 + core),
            )
    last = chips - 1
    down(tp)
    arrive(pair_in.at[last], pr_r.at[last], pr_s.at[last])
    for k in list(range(1, groups)) + [0]:
        s = lax.rem(ep + k, groups)
        term = po[tp, s].astype(jnp.float32) + pair_in[last, s].astype(jnp.float32)
        for i in range(chips - 1):
            arrive(y_in.at[i, s], yr_r.at[i, k], yr_s.at[i, k])
            term = term + y_in[i, s].astype(jnp.float32)
        if k > 0:
            ret_out[s] = term.astype(jnp.bfloat16)
            send(ret_out.at[s], ret_in.at[ep], rt_s.at[k], rt_r.at[k], (s, tp))
        else:
            ret_in[s] = term.astype(jnp.bfloat16)
    for k in range(1, groups):
        src = lax.rem(ep + groups - k, groups)
        arrive(ret_in.at[src], rt_r.at[k], rt_s.at[k])

    back = ret_in[...].reshape(slots, share)
    high = blend.astype(jnp.bfloat16)
    low = (blend - high.astype(jnp.float32)).astype(jnp.bfloat16)
    dims = (((0,), (0,)), ((), ()))
    routed = lax.dot_general(high, back, dims, preferred_element_type=jnp.float32)
    routed = routed + lax.dot_general(low, back, dims, preferred_element_type=jnp.float32)
    out_ref[...] = (res_scr[...].astype(jnp.float32) + routed).astype(jnp.bfloat16)
    for copy in sends:
        copy.wait_send()


def expert_step(tokens, mixed, gain, routing, route_weight, wo, wg, wu, wd):
    groups, tp_width = lax.axis_size("ep"), lax.axis_size("tp")
    rows, model = tokens.shape
    share = model // tp_width
    chips = tp_width // 2
    need = 2 * rows * routing.shape[0] // groups
    capacity = -(-need // 16) * 16
    slots = groups * capacity
    ff = wg.shape[1]
    bf16, f32 = jnp.bfloat16, jnp.float32
    wg, wu, wd = [pltpu.with_memory_space_constraint(a, pltpu.HBM) for a in (wg, wu, wd)]
    vmem = pl.BlockSpec(memory_space=pltpu.VMEM)
    hbm = pl.BlockSpec(memory_space=pltpu.HBM)
    block = (groups, capacity, share)
    sem = pltpu.SemaphoreType.DMA
    return pl.pallas_call(
        functools.partial(expert_kernel, groups, tp_width, capacity),
        out_shape=jax.ShapeDtypeStruct((rows, share), bf16),
        in_specs=[vmem] * 6 + [hbm] * 3,
        out_specs=vmem,
        scratch_shapes=[
            pltpu.VMEM(wg.shape, bf16),
            pltpu.VMEM(wu.shape, bf16), pltpu.VMEM(wd.shape, bf16),
            pltpu.VMEM(gain.shape, f32),
            pltpu.VMEM((tp_width, rows, share), bf16),
            pltpu.VMEM((tp_width, rows, share), bf16),
            pltpu.VMEM((1, 128), f32),
            pltpu.VMEM((tp_width, 1, 128), f32),
            pltpu.VMEM((1, slots), f32),
            pltpu.VMEM((groups, 1, slots), f32),
            pltpu.VMEM(block, bf16),
            pltpu.VMEM((tp_width,) + block, bf16),
            pltpu.VMEM((tp_width,) + block, bf16),
            pltpu.VMEM((chips,) + block, bf16),
            pltpu.VMEM((chips,) + block, bf16),
            pltpu.VMEM((chips,) + block, bf16),
            pltpu.VMEM(block, bf16),
            pltpu.VMEM(block, bf16),
            pltpu.VMEM((rows, share), bf16),
            pltpu.VMEM((slots, ff), f32),
            pltpu.VMEM((slots, ff), f32),
            sem((3,)),
            sem((tp_width,)), sem((tp_width,)),
            sem((tp_width,)), sem((tp_width,)),
            sem((groups,)), sem((groups,)),
            sem((groups,)), sem((groups,)),
            sem((chips, groups)), sem((chips, groups)),
            sem((chips, groups)), sem((chips, groups)),
            sem((chips,)), sem((chips,)),
            sem((chips, groups)), sem((chips, groups)),
            sem((groups,)), sem((groups,)),
        ],
        compiler_params=pltpu.CompilerParams(
            collective_id=0, has_side_effects=True, vmem_limit_bytes=EXPERT_VMEM
        ),
        name="experts",
    )(mixed, tokens, gain, routing, route_weight, wo, wg, wu, wd)


def on_device(
    tokens,
    mix_gain,
    query_weight,
    key_weight,
    value_weight,
    decay_weight,
    strength_weight,
    decay_rate,
    head_gain,
    memory_state,
    output_weight,
    ffn_gain,
    routing,
    route_weight,
    expert_gate,
    expert_up,
    expert_down,
):
    mixed, new_state = mix_step(
        tokens, mix_gain.reshape(-1, 128), query_weight, key_weight, value_weight,
        decay_weight.T, strength_weight.T, decay_rate[None, :], head_gain[None, :], memory_state,
    )
    layer_out = expert_step(
        tokens, mixed, ffn_gain.reshape(-1, 128), routing.T, route_weight.T, output_weight,
        expert_gate[0], expert_up[0], expert_down[0],
    )
    return (layer_out, new_state)


def solution(mesh):
    placed = (
        P("ep", None),
        P(),
        P(None, "tp"),
        P(None, "tp"),
        P(None, "tp"),
        P(),
        P(),
        P("tp"),
        P(),
        P("ep", "tp", None, None),
        P("tp", None),
        P(),
        P("ep", None),
        P("ep", None),
        P("ep", None, "tp"),
        P("ep", None, "tp"),
        P("ep", "tp", None),
    )
    return jax.shard_map(
        on_device,
        mesh=mesh,
        in_specs=placed,
        out_specs=(P("ep", "tp"), P("ep", "tp", None, None)),
        check_vma=False,
    )
```

time: 58.4 us -> 47.2 us (0.81)
  local copies, waits for them, and re-layouts: 6.8 us -> 0.65 us
  Pallas kernels: 50.6 us -> 45.7 us
    pallas_call x1, Pallas kernels: 40 us -> 36.4 us  [expert_step(): pl.pallas_call(functools.partial(expert_kernel, groups, tp_width, capacit...]
    unnamed x3 -> x11, local copies, waits for them, and re-layouts: 4.19 us -> 0.65 us
    broadcast_in_dim x2 -> x0, local copies, waits for them, and re-layouts: 2.62 us -> none  [the longest x1 1.31 us: on_device(): mix_gain[None, :]]
    pallas_call x1, Pallas kernels: 10.6 us -> 9.35 us  [mix_step(): pl.pallas_call(mix_kernel, out_shape=(jax.ShapeDtypeStruct((rows, inner),...]
where the time goes in v1:
time: 47.2 us; the launch traced here: 47.1 us
  Pallas kernels  45.7 us (97%)
  between operations  0.73 us (2%)
  local copies, waits for them, and re-layouts  0.65 us (1%)
    pallas_call x1, Pallas kernels, expert_step(): pl.pallas_call(functools.partial(expert_kernel, groups, tp_width, capacit...  36.4 us
    pallas_call x1, Pallas kernels, mix_step(): pl.pallas_call(mix_kernel, out_shape=(jax.ShapeDtypeStruct((rows, inner),...  9.35 us

profile of v1, /device:TPU:0, one launch (start us, length us, event | category | flops | bytes accessed | tf_op | source)
XLA Modules:
  0.0 47.1 jit_solution(10264621149929511486)
XLA Ops:
  0.6 0.0 copy-start
  0.6 0.0 copy-start.1
  0.7 0.0 copy-start.2
  0.7 0.0 copy-start.3
  0.7 0.0 copy-start.4
  0.7 9.4 %mix.1 = (bf16[32,256]{1,0:T(8,128)(2,1)S(1)}, f32[32,2,128,128]{3,2,1,0:T(8,128)}) custom-call(bf16[32,4096]{1,0:T(8,128)(2,1)} %tok_ref.1, bf16[32,128]{1,0:T(8,128)(2,1)} %bitcast.19, bf16[8,4096]{1,0:T(8,128)(2,1)} %bitcast.17, bf16[8,4096]{1,0:T(8,128)(2,1)} %bitcast.18, f32[1,2]{1,0:T(1,128)} %bitcast.20, bf16[1,128]{1,0:T(2,128)(2,1)} %bitcast.21, ...), custom_call_target="tpu_custom_call" | custom-call | tf_op jit(solution)/shard_map/mix/pallas_call | solution.py:153
  10.0 0.0 copy-done
  10.1 0.0 copy-done.1
  10.1 0.0 copy-done.2
  10.1 0.0 copy-done.3
  10.1 0.0 copy-done.4
  10.1 36.4 %experts.1 = bf16[32,1024]{1,0:T(8,128)(2,1)S(1)} custom-call(bf16[32,256]{1,0:T(8,128)(2,1)S(1)} %get-tuple-element.4.mixed_ref, bf16[32,4096]{1,0:T(8,128)(2,1)S(1)} %copy-done.1, bf16[32,128]{1,0:T(8,128)(2,1)S(1)} %bitcast.11, s32[2,32]{1,0:T(2,128)S(1)} %bitcast.12, f32[2,32]{1,0:T(2,128)S(1)} %bitcast.13, bf16[256,4096]{1,0:T(8,128)(2,1)S(1)} %copy-done, ...), custom_call_target="tpu_custom_call" | custom-call | tf_op jit(solution)/shard_map/experts/pallas_call | solution.py:441
  46.5 0.6 %copy.20 = bf16[32,1024]{1,0:T(8,128)(2,1)} copy(bf16[32,1024]{1,0:T(8,128)(2,1)S(1)} %experts.1) | data formatting | bytes 131072
Async XLA Ops:
  0.6 9.4 %copy-start = (bf16[256,4096]{1,0:T(8,128)(2,1)S(1)}, bf16[256,4096]{1,0:T(8,128)(2,1)}, u32[]{:S(2)}) copy-start(bf16[256,4096]{1,0:T(8,128)(2,1)} %wo.1) | copy-start | bytes 6291460
  0.6 9.4 %copy-start.1 = (bf16[32,4096]{1,0:T(8,128)(2,1)S(1)}, bf16[32,4096]{1,0:T(8,128)(2,1)}, u32[]{:S(2)}) copy-start(bf16[32,4096]{1,0:T(8,128)(2,1)} %tok_ref.1) | copy-start | bytes 786436
  0.7 9.4 %copy-start.2 = (bf16[4096]{0:T(1024)(128)(2,1)S(1)}, bf16[4096]{0:T(1024)(128)(2,1)}, u32[]{:S(2)}) copy-start(bf16[4096]{0:T(1024)(128)(2,1)} %param.28) | copy-start | bytes 24580
  0.7 9.4 %copy-start.3 = (s32[32,2]{0,1:T(2,128)S(1)}, s32[32,2]{0,1:T(2,128)}, u32[]{:S(2)}) copy-start(s32[32,2]{0,1:T(2,128)} %param.29) | copy-start | bytes 772
  0.7 9.4 %copy-start.4 = (f32[32,2]{0,1:T(2,128)S(1)}, f32[32,2]{0,1:T(2,128)}, u32[]{:S(2)}) copy-start(f32[32,2]{0,1:T(2,128)} %param.30) | copy-start | bytes 772
